TPU v7x, 32 devices: a whole 2x2x4 slice. The times are simulated.
32 devices in a mesh: sp: 8 (over z, y), tp: 4 (over x, core).
Axes of the slice: x: 2, y: 2, z: 4, core: 2. Of those that a mesh axis runs over, the one named last changes fastest.
Arguments:
- target: bfloat16 [2048, 2048], P(('sp', 'tp')), may hold values from -6 to 6
- source: bfloat16 [4096, 2048], P(('sp', 'tp')), may hold values from -6 to 6
- target_gain: bfloat16 [2, 2048], replicated, may hold values from 0.099609375 to 1.8984375
- source_gain: bfloat16 [2, 2048], replicated, may hold values from 0.099609375 to 1.8984375
- query_w: bfloat16 [2, 2048, 8192], P(None, None, 'tp'), may hold values from -0.125 to 0.125
- key_w: bfloat16 [2, 2048, 4096], P(None, None, 'tp'), may hold values from -0.125 to 0.125
- value_w: bfloat16 [2, 2048, 4096], P(None, None, 'tp'), may hold values from -0.125 to 0.125
- out_w: bfloat16 [2, 8192, 2048], P(None, 'tp'), may hold values from -0.1875 to 0.1875
- head_temp: float32 [2, 16], P(None, 'tp'), may hold values from 1.5 to 8, as said below
- final_gain: bfloat16 [2048], replicated, may hold values from 0.099609375 to 1.8984375
Outputs:
- result: float32 [2048, 2048], P(('sp', 'tp'))
Inputs may be any that keep to these rules, and one draw needn't show every extreme that they name: `head_temp`: a positive scale for each head's scores.
All inputs are finite; a program needn't handle non-finite values.
Results may differ from a plain program's by a relative error of at most 0.04.
Values may be sent and summed in bfloat16 or wider, within the bound.
A program may use at most 192 MiB of HBM per device.

v0:
```python
import jax
import jax.numpy as jnp
from jax import lax
from jax.sharding import PartitionSpec as P

HEAD_DIM = 512


EPS = 1e-06
FLOOR = -1e30


def unit_rows(matrix):
    values = matrix.astype(jnp.float32)
    return values * lax.rsqrt(jnp.mean(values * values, axis=-1, keepdims=True) + EPS)


def per_device(
    target, source, target_gain, source_gain, query_w, key_w, value_w, out_w, head_temp, final_gain
):
    local_heads = query_w.shape[2] // HEAD_DIM
    local_shared = key_w.shape[2] // HEAD_DIM
    group_size = local_heads // local_shared
    shared_width = key_w.shape[2]
    source_gains = source_gain.astype(jnp.float32)
    unit_piece = unit_rows(lax.all_gather(source, "tp", axis=0, tiled=True))
    outputs = []
    for project_layer_index in range(2):
        project_normed = (unit_piece * source_gains[project_layer_index]).astype(jnp.bfloat16)
        outputs.append(
            jnp.dot(
                project_normed, key_w[project_layer_index], preferred_element_type=jnp.float32
            ).astype(jnp.bfloat16)
        )
        outputs.append(
            jnp.dot(
                project_normed, value_w[project_layer_index], preferred_element_type=jnp.float32
            ).astype(jnp.bfloat16)
        )
    projected = jnp.concatenate(outputs, axis=1)
    hidden_state = target.astype(jnp.float32)
    for layer_index in range(2):
        key_rows = projected[
            :, 2 * layer_index * shared_width : (2 * layer_index + 1) * shared_width
        ]
        value_rows = projected[
            :, (2 * layer_index + 1) * shared_width : (2 * layer_index + 2) * shared_width
        ]
        normed = (unit_rows(hidden_state) * target_gain[layer_index].astype(jnp.float32)).astype(
            jnp.bfloat16
        )
        queries = jnp.dot(
            lax.all_gather(normed, "tp", axis=0, tiled=True),
            query_w[layer_index],
            preferred_element_type=jnp.float32,
        ).astype(jnp.bfloat16)
        row_count = queries.shape[0]
        query_view = queries.reshape(row_count, local_shared, group_size, HEAD_DIM)
        scales = (head_temp[layer_index] * HEAD_DIM ** (-0.5)).reshape(local_shared, group_size)
        start_max = jnp.full((row_count, local_shared, group_size), FLOOR, jnp.float32)
        row_max = start_max
        key_view = lax.all_gather(key_rows, "sp", axis=0, tiled=True).reshape(
            -1, local_shared, HEAD_DIM
        )
        value_view = lax.all_gather(value_rows, "sp", axis=0, tiled=True).reshape(
            -1, local_shared, HEAD_DIM
        )
        scores = jnp.einsum(
            "tkgd,nkd->tkgn", query_view, key_view, preferred_element_type=jnp.float32
        )
        scores = scores * scales[None, :, :, None]
        new_max = jnp.maximum(row_max, jnp.max(scores, axis=-1))
        exponent = jnp.exp(scores - new_max[..., None])
        row_total = jnp.sum(exponent, axis=-1)
        accumulated = jnp.einsum(
            "tkgn,nkd->tkgd",
            exponent.astype(jnp.bfloat16),
            value_view,
            preferred_element_type=jnp.float32,
        )
        row_max, row_total, accumulated = (new_max, row_total, accumulated)
        attended = (accumulated / row_total[..., None]).astype(jnp.bfloat16)
        flat_heads = attended.reshape(row_count, local_heads * HEAD_DIM)
        mixed = lax.psum_scatter(
            jnp.dot(flat_heads, out_w[layer_index], preferred_element_type=jnp.float32).astype(
                jnp.bfloat16
            ),
            "tp",
            scatter_dimension=0,
            tiled=True,
        ).astype(jnp.float32)
        hidden_state = hidden_state + mixed
    return unit_rows(hidden_state) * final_gain.astype(jnp.float32)


def solution(mesh):
    in_specs = (
        P(("sp", "tp"), None),
        P(("sp", "tp"), None),
        P(),
        P(),
        P(None, None, "tp"),
        P(None, None, "tp"),
        P(None, None, "tp"),
        P(None, "tp", None),
        P(None, "tp"),
        P(),
    )
    out_specs = P(("sp", "tp"), None)
    return jax.shard_map(
        per_device, mesh=mesh, in_specs=in_specs, out_specs=out_specs, check_vma=False
    )
```

profile of v0, /device:TPU:0, one launch (start us, length us, event | category | flops | bytes accessed | tf_op | source)
XLA Modules:
  0.0 709.3 jit_solution(11185202553054778158)
XLA Ops:
  6.5 0.0 all-gather.8.cloned.1.call-start
  6.5 0.7 all-gather.8.cloned.1.call-update
  7.3 0.0 all-gather.14.cloned.1.call-start
  7.3 1.1 fusion.83
  8.4 0.8 slice_convert_fusion
  9.2 1.8 fusion.85
  11.0 0.0 all-gather.14.cloned.1.call-update
  11.0 0.0 all-gather.12.cloned.1.call-start
  11.1 0.8 fusion.86
  11.9 22.3 %all-gather.8.cloned.1.call-done = bf16[512,2048]{1,0:T(8,128)(2,1)} async-done(((bf16[128,2048]{1,0:T(8,128)(2,1)}), bf16[512,2048]{1,0:T(8,128)(2,1)}) %all-gather.8.cloned.1.call-update) | async-done | bytes 2097168 | tf_op jit(solution)/shard_map/all_gather | solution.py:26
  34.2 2.1 fusion.34
  36.3 6.3 fusion.68
  42.6 0.0 all-gather.12.cloned.1.call-update
  42.6 0.0 copy-start.4
  42.7 0.0 all-gather.10.cloned.1.call-start
  42.7 0.0 copy-done.2
  42.7 5.7 fusion.65
  48.4 0.0 all-gather.10.cloned.1.call-update
  48.4 0.3 reduce-scatter.3.cloned.1.call-start
  48.8 0.0 copy-done.4
  48.8 0.1 mul.154
  48.9 3.6 all-gather.14.cloned.1.call-done
  52.5 7.1 %fusion.47 = bf16[256,2048]{1,0:T(8,128)(2,1)} fusion(bf16[256,2048]{1,0:T(8,128)(2,1)} %all-gather.14.cloned.1.call-done, bf16[2,2048,2048]{2,1,0:T(8,128)(2,1)} %param.14), kind=kOutput, calls=%fused_computation.51 | convolution fusion | flops 2148007936 | bytes 10485760 | tf_op jit(solution)/shard_map/dot_general | solution.py:52
  59.6 1.8 reshape.81
  61.4 117.7 %all-gather.12.cloned.1.call-done = bf16[4096,1024]{1,0:T(8,128)(2,1)} async-done(((bf16[512,1024]{1,0:T(8,128)(2,1)}), bf16[4096,1024]{1,0:T(8,128)(2,1)}) %all-gather.12.cloned.1.call-update) | async-done | bytes 8388624 | tf_op jit(solution)/shard_map/all_gather | solution.py:62
  179.1 14.7 %reshape.80 = bf16[4096,2,512]{2,1,0:T(2,128)(2,1)} reshape(bf16[4096,1024]{1,0:T(8,128)(2,1)} %all-gather.12.cloned.1.call-done) | data formatting | bytes 16777216 | tf_op jit(solution)/shard_map/reshape | solution.py:62
  193.8 12.6 %bitcast_reduce_fusion.1 = (f32[256,2,2]{0,2,1:T(2,128)S(1)}, f32[2,4096,256,2]{2,1,3,0:T(8,128)}) fusion(f32[2,2]{1,0:T(2,128)S(1)} %mul.154, bf16[256,2,2,512]{3,2,1,0:T(2,128)(2,1)S(1)} %reshape.81, bf16[4096,2,512,1]{2,1,0,3:T(2,128)(2,1)} %bitcast.99), kind=kOutput, calls=%fused_computation.4 | convolution fusion | flops 4303354880 | bytes 26218512 | tf_op jit(solution)/shard_map/tkgd,nkd->tkgn/dot_general | solution.py:68
  206.4 8.6 %fusion.2 = f32[256,2,2]{0,2,1:T(2,128)S(1)} fusion(f32[2,4096,256,2]{2,1,3,0:T(8,128)} %get-tuple-element.12, f32[256,2,2]{0,2,1:T(2,128)S(1)} %broadcast_maximum_fusion.1, f32[2,2]{1,0:T(2,128)S(1)} %mul.154), kind=kLoop, calls=%fused_computation.6 | loop fusion | flops 12581888 | bytes 16785424 | tf_op jit(solution)/shard_map/reduce_sum | solution.py:74
  215.0 88.8 %all-gather.10.cloned.1.call-done = bf16[4096,1024]{1,0:T(8,128)(2,1)} async-done(((bf16[512,1024]{1,0:T(8,128)(2,1)}), bf16[4096,1024]{1,0:T(8,128)(2,1)}) %all-gather.10.cloned.1.call-update) | async-done | bytes 8388624 | tf_op jit(solution)/shard_map/all_gather | solution.py:65
  303.8 12.3 %copy.25 = bf16[4096,1024]{0,1:T(8,128)(2,1)} copy(bf16[4096,1024]{1,0:T(8,128)(2,1)} %all-gather.10.cloned.1.call-done) | data formatting | bytes 16777216 | tf_op jit(solution)/shard_map/reshape | solution.py:65
  316.2 12.8 %fusion.60 = bf16[256,2,2,512]{0,3,2,1:T(8,128)(2,1)S(1)} fusion(bf16[4096,2,512,1]{0,2,3,1:T(8,128)(2,1)} %bitcast.98, f32[2,4096,256,2]{2,1,3,0:T(8,128)} %get-tuple-element.12, f32[256,2,2]{0,2,1:T(2,128)S(1)} %broadcast_maximum_fusion.1, f32[2,2]{1,0:T(2,128)S(1)} %mul.154, f32[256,2,2]{0,2,1:T(2,128)S(1)} %fusion.2), kind=kOutput, calls=%fused_computation.58 | convolution fusion | flops 4308598784 | bytes 26222608 | tf_op jit(solution)/shard_map/tkgn,nkd->tkgd/dot_general | solution.py:75
  329.0 6.7 fusion.50
  335.7 0.0 reduce-scatter.3.cloned.1.call-update
  335.7 0.0 all-gather.18.cloned.1.call-start
  335.8 5.6 fusion.74
  341.4 0.0 all-gather.18.cloned.1.call-update
  341.4 0.0 copy-start
  341.4 0.0 all-gather.16.cloned.1.call-start
  341.5 5.7 fusion.71
  347.2 0.0 all-gather.16.cloned.1.call-update
  347.2 0.0 all-gather.20.cloned.1.call-start
  347.3 11.6 %reduce-scatter.3.cloned.1.call-done = bf16[64,2048]{1,0:T(8,128)(2,1)} async-done(((bf16[256,2048]{1,0:T(8,128)(2,1)}), bf16[64,2048]{1,0:T(8,128)(2,1)}) %reduce-scatter.3.cloned.1.call-update) | async-done | bytes 262160 | tf_op jit(solution)/shard_map/reduce_scatter | solution.py:84
  358.9 1.1 multiply_reduce_fusion.1
  360.0 1.8 multiply_convert_fusion
  361.8 0.0 all-gather.20.cloned.1.call-update
  361.8 0.0 reduce-scatter.5.cloned.1.call-start
  361.9 0.1 mul.169
  362.0 123.4 %all-gather.18.cloned.1.call-done = bf16[4096,1024]{1,0:T(8,128)(2,1)} async-done(((bf16[512,1024]{1,0:T(8,128)(2,1)}), bf16[4096,1024]{1,0:T(8,128)(2,1)}) %all-gather.18.cloned.1.call-update) | async-done | bytes 8388624 | tf_op jit(solution)/shard_map/all_gather | solution.py:62
  485.3 14.8 %reshape.84 = bf16[4096,2,512]{2,1,0:T(2,128)(2,1)} reshape(bf16[4096,1024]{1,0:T(8,128)(2,1)} %all-gather.18.cloned.1.call-done) | data formatting | bytes 16777216 | tf_op jit(solution)/shard_map/reshape | solution.py:62
  500.1 110.1 %all-gather.16.cloned.1.call-done = bf16[4096,1024]{1,0:T(8,128)(2,1)} async-done(((bf16[512,1024]{1,0:T(8,128)(2,1)}), bf16[4096,1024]{1,0:T(8,128)(2,1)}) %all-gather.16.cloned.1.call-update) | async-done | bytes 8388624 | tf_op jit(solution)/shard_map/all_gather | solution.py:65
  610.2 11.9 %copy.28 = bf16[4096,1024]{0,1:T(8,128)(2,1)} copy(bf16[4096,1024]{1,0:T(8,128)(2,1)} %all-gather.16.cloned.1.call-done) | data formatting | bytes 16777216 | tf_op jit(solution)/shard_map/reshape | solution.py:65
  622.0 4.6 all-gather.20.cloned.1.call-done
  626.6 6.0 fusion.53
  632.7 0.8 reshape.85
  633.5 12.7 %bitcast_reduce_fusion = (f32[256,2,2]{0,2,1:T(2,128)S(1)}, f32[2,4096,256,2]{2,1,3,0:T(8,128)}) fusion(f32[2,2]{1,0:T(2,128)S(1)} %mul.169, bf16[256,2,2,512]{3,2,1,0:T(2,128)(2,1)S(1)} %reshape.85, bf16[4096,2,512,1]{2,1,0,3:T(2,128)(2,1)} %bitcast.97), kind=kOutput, calls=%fused_computation.1 | convolution fusion | flops 4303354880 | bytes 26218512 | tf_op jit(solution)/shard_map/tkgd,nkd->tkgn/dot_general | solution.py:68
  646.2 8.6 %fusion.4 = f32[256,2,2]{0,2,1:T(2,128)S(1)} fusion(f32[2,4096,256,2]{2,1,3,0:T(8,128)} %get-tuple-element.14, f32[256,2,2]{0,2,1:T(2,128)S(1)} %broadcast_maximum_fusion, f32[2,2]{1,0:T(2,128)S(1)} %mul.169), kind=kLoop, calls=%fused_computation.8 | loop fusion | flops 12581888 | bytes 16785424 | tf_op jit(solution)/shard_map/reduce_sum | solution.py:74
  654.8 12.9 %fusion.59 = bf16[256,2,2,512]{0,3,2,1:T(8,128)(2,1)S(1)} fusion(bf16[4096,2,512,1]{0,2,3,1:T(8,128)(2,1)} %bitcast.96, f32[2,4096,256,2]{2,1,3,0:T(8,128)} %get-tuple-element.14, f32[256,2,2]{0,2,1:T(2,128)S(1)} %broadcast_maximum_fusion, f32[2,2]{1,0:T(2,128)S(1)} %mul.169, f32[256,2,2]{0,2,1:T(2,128)S(1)} %fusion.4), kind=kOutput, calls=%fused_computation.56 | convolution fusion | flops 4308598784 | bytes 26222608 | tf_op jit(solution)/shard_map/tkgn,nkd->tkgd/dot_general | solution.py:75
  667.6 0.0 copy-start.3
  667.7 6.8 fusion.56
  674.4 0.0 reduce-scatter.5.cloned.1.call-update
  674.5 0.0 copy-done.3
  674.5 25.0 %reduce-scatter.5.cloned.1.call-done = bf16[64,2048]{1,0:T(8,128)(2,1)} async-done(((bf16[256,2048]{1,0:T(8,128)(2,1)}), bf16[64,2048]{1,0:T(8,128)(2,1)}) %reduce-scatter.5.cloned.1.call-update) | async-done | bytes 262160 | tf_op jit(solution)/shard_map/reduce_scatter | solution.py:84
  699.4 1.2 multiply_reduce_fusion
  700.6 1.9 multiply_multiply_fusion
  (12 shorter events, 0.1 us)
Async XLA Ops:
  6.5 27.7 %all-gather.8.cloned.1.call-start = ((), (), s32[]{:S(2)}) async-start(), calls=%async_computation.2 | async-start | bytes 2621440 | tf_op jit(solution)/shard_map/all_gather | solution.py:26
  7.3 45.2 %all-gather.14.cloned.1.call-start = ((), (), s32[]{:S(2)}) async-start(), calls=%async_computation.5 | async-start | bytes 1310720 | tf_op jit(solution)/shard_map/all_gather | solution.py:53
  11.0 168.1 %all-gather.12.cloned.1.call-start = ((), (), s32[]{:S(2)}) async-start(), calls=%async_computation.4 | async-start | bytes 9437184 | tf_op jit(solution)/shard_map/all_gather | solution.py:62
  36.3 6.4 copy-start.2
  42.6 6.1 copy-start.4
  42.7 261.2 %all-gather.10.cloned.1.call-start = ((), (), s32[]{:S(2)}) async-start(), calls=%async_computation.3 | async-start | bytes 9437184 | tf_op jit(solution)/shard_map/all_gather | solution.py:65
  48.4 310.4 %reduce-scatter.3.cloned.1.call-start = ((), (), s32[]{:S(2)}) async-start(), calls=%async_computation.6 | async-start | bytes 1310720 | tf_op jit(solution)/shard_map/reduce_scatter | solution.py:84
  335.7 149.6 %all-gather.18.cloned.1.call-start = ((), (), s32[]{:S(2)}) async-start(), calls=%async_computation.8 | async-start | bytes 9437184 | tf_op jit(solution)/shard_map/all_gather | solution.py:62
  341.4 17.5 %copy-start = (bf16[64,2048]{1,0:T(8,128)(2,1)S(1)}, bf16[64,2048]{1,0:T(8,128)(2,1)}, u32[]{:S(2)}) copy-start(bf16[64,2048]{1,0:T(8,128)(2,1)} %param.10) | copy-start | bytes 786436
  341.4 268.7 %all-gather.16.cloned.1.call-start = ((), (), s32[]{:S(2)}) async-start(), calls=%async_computation.7 | async-start | bytes 9437184 | tf_op jit(solution)/shard_map/all_gather | solution.py:65
  347.2 279.4 %all-gather.20.cloned.1.call-start = ((), (), s32[]{:S(2)}) async-start(), calls=%async_computation.9 | async-start | bytes 1310720 | tf_op jit(solution)/shard_map/all_gather | solution.py:53
  361.8 337.6 %reduce-scatter.5.cloned.1.call-start = ((), (), s32[]{:S(2)}) async-start(), calls=%async_computation.10 | async-start | bytes 1310720 | tf_op jit(solution)/shard_map/reduce_scatter | solution.py:84
  667.6 6.8 copy-start.3
  667.7 31.8 %copy-start.1 = (bf16[64,2048]{1,0:T(8,128)(2,1)S(1)}, bf16[64,2048]{1,0:T(8,128)(2,1)}, u32[]{:S(2)}) copy-start(bf16[64,2048]{1,0:T(8,128)(2,1)} %reduce-scatter.3.cloned.1.call-done) | copy-start | bytes 786436
Sparse Core Ops, SparseCore 0:
  8.9 25.2 all-gather.7
  35.8 16.6 all-gather.13
  54.6 124.4 all-gather.11
  181.1 122.6 all-gather.9
  335.9 22.9 reduce-scatter.2
  360.8 124.4 all-gather.17
  487.5 122.6 all-gather.15
  611.7 14.8 all-gather.19
  674.6 24.8 reduce-scatter.4
where the time goes:
time: 715 us; the launch traced here: 709 us
  waiting for transfers between devices  508 us (71%)
  matrix products  101 us (14%)
  local copies, waits for them, and re-layouts  57.2 us (8%)
  other arithmetic  29 us (4%)
  between operations  13.6 us (2%)
    all_gather x2, waiting for transfers between devices, per_device(): lax.all_gather(key_rows, 'sp', axis=0, tiled=True)  241 us
    all_gather x2, waiting for transfers between devices, per_device(): lax.all_gather(value_rows, 'sp', axis=0, tiled=True)  199 us
    reduce_scatter x2, waiting for transfers between devices, per_device(): lax.psum_scatter(jnp.dot(flat_heads, out_w[layer_index], preferred_elemen...  36.5 us
    reshape x2, local copies, waits for them, and re-layouts, per_device(): lax.all_gather(key_rows, 'sp', axis=0, tiled=True)  29.4 us
    dot_general x2, matrix products, per_device(): jnp.einsum('tkgn,nkd->tkgd', exponent.astype(jnp.bfloat16), value_view, p...  25.7 us
    dot_general x2, matrix products, per_device(): jnp.einsum('tkgd,nkd->tkgn', query_view, key_view, preferred_element_type...  25.3 us
    reshape x2, local copies, waits for them, and re-layouts, per_device(): lax.all_gather(value_rows, 'sp', axis=0, tiled=True)  24.2 us
    all_gather x1, waiting for transfers between devices, per_device(): unit_piece = unit_rows(lax.all_gather(source, 'tp', axis=0, tiled=True))  22.3 us
  transfers between devices with their start and end apart: 9, of which 9 were waited for; matrix products, arithmetic and copies ran while one was open for 15% of the time, Pallas kernels for 0%

commit v1 on v0

v1 whole, which is shorter than its diff:
```python
import functools
import math

import jax
import jax.numpy as jnp
from jax import lax
from jax.experimental import pallas as pl
from jax.experimental.pallas import tpu as pltpu
from jax.sharding import PartitionSpec as P

HEAD_DIM = 512
EPS = 1e-06
FLOOR = -1e30
CHUNK = 512
ROWS = 512
LOG2E = math.log2(math.e)


def unit_rows(matrix):
    values = matrix.astype(jnp.float32)
    return values * lax.rsqrt(jnp.mean(values * values, axis=-1, keepdims=True) + EPS)


def attend_kernel(rows, query_ref, source_ref, mix_ref, total_ref, top_ref, sum_ref):
    step = pl.program_id(0)
    count = query_ref.shape[0]

    @pl.when(step == 0)
    def _():
        total_ref[...] = jnp.zeros_like(total_ref)
        sum_ref[...] = jnp.zeros_like(sum_ref)
        top_ref[...] = jnp.full_like(top_ref, FLOOR)

    for start in range(0, count, rows):
        block = pl.ds(start, rows)
        scores = lax.dot_general(
            query_ref[block, :],
            source_ref[...],
            (((1,), (1,)), ((), ())),
            preferred_element_type=jnp.float32,
        )
        old_top = top_ref[block, :1]
        new_top = jnp.maximum(old_top, jnp.max(scores, axis=-1, keepdims=True))
        shrink = jnp.exp2(old_top - new_top)
        expo = jnp.exp2(scores - new_top)
        top_ref[block, :] = jnp.broadcast_to(new_top, (rows, top_ref.shape[1]))
        new_sum = sum_ref[block, :1] * shrink + jnp.sum(expo, axis=-1, keepdims=True)
        sum_ref[block, :] = jnp.broadcast_to(new_sum, (rows, sum_ref.shape[1]))
        total_ref[block, :] = total_ref[block, :] * shrink + jnp.dot(
            expo.astype(jnp.bfloat16), source_ref[...], preferred_element_type=jnp.float32
        )

    @pl.when(step == pl.num_programs(0) - 1)
    def _():
        for start in range(0, count, rows):
            block = pl.ds(start, rows)
            mix_ref[block, :] = (total_ref[block, :] / sum_ref[block, :1]).astype(mix_ref.dtype)


def attend(query, source, chunk=CHUNK, rows=ROWS):
    count, width = query.shape
    positions = source.shape[0]
    chunk = math.gcd(chunk, positions)
    rows = math.gcd(rows, count)
    return pl.pallas_call(
        functools.partial(attend_kernel, rows),
        grid=(positions // chunk,),
        out_shape=jax.ShapeDtypeStruct((count, width), jnp.bfloat16),
        in_specs=[
            pl.BlockSpec((count, width), lambda j: (0, 0), pipeline_mode=pl.Buffered(1)),
            pl.BlockSpec((chunk, width), lambda j: (j, 0)),
        ],
        out_specs=pl.BlockSpec((count, width), lambda j: (0, 0), pipeline_mode=pl.Buffered(1)),
        scratch_shapes=[
            pltpu.VMEM((count, width), jnp.float32),
            pltpu.VMEM((count, 128), jnp.float32),
            pltpu.VMEM((count, 128), jnp.float32),
        ],
        compiler_params=pltpu.CompilerParams(
            dimension_semantics=("arbitrary",), vmem_limit_bytes=56 * 1024 * 1024
        ),
        cost_estimate=pl.CostEstimate(
            flops=4 * count * positions * width,
            bytes_accessed=2 * positions * width,
            transcendentals=count * positions,
        ),
    )(query, source)


def per_device(
    target, source, target_gain, source_gain, query_w, key_w, value_w, out_w, head_temp, final_gain
):
    width = target.shape[1]
    heads = query_w.shape[2] // HEAD_DIM
    shared = key_w.shape[2] // HEAD_DIM
    group = heads // shared
    positions = lax.all_gather(
        unit_rows(source).astype(jnp.bfloat16), ("sp", "tp"), axis=0, tiled=True
    )
    hidden_state = target.astype(jnp.float32)
    for layer in range(2):
        gain = source_gain[layer].astype(jnp.float32)
        normed = (unit_rows(hidden_state) * target_gain[layer].astype(jnp.float32)).astype(
            jnp.bfloat16
        )
        queries = jnp.dot(
            lax.all_gather(normed, "tp", axis=0, tiled=True),
            query_w[layer],
            preferred_element_type=jnp.float32,
        ).astype(jnp.bfloat16)
        count = queries.shape[0]
        scales = head_temp[layer] * (HEAD_DIM ** (-0.5) * LOG2E)
        lifted = []
        for head in range(heads):
            columns = slice((head // group) * HEAD_DIM, (head // group + 1) * HEAD_DIM)
            lifted.append(
                (
                    lax.dot_general(
                        queries[:, head * HEAD_DIM : (head + 1) * HEAD_DIM],
                        key_w[layer][:, columns],
                        (((1,), (1,)), ((), ())),
                        preferred_element_type=jnp.float32,
                    )
                    * (gain * scales[head])
                ).astype(jnp.bfloat16)
            )
        mix = attend(jnp.concatenate(lifted, axis=0), positions)
        attended = []
        for head in range(heads):
            columns = slice((head // group) * HEAD_DIM, (head // group + 1) * HEAD_DIM)
            own = (mix[head * count : (head + 1) * count].astype(jnp.float32) * gain).astype(
                jnp.bfloat16
            )
            attended.append(
                jnp.dot(
                    own, value_w[layer][:, columns], preferred_element_type=jnp.float32
                ).astype(jnp.bfloat16)
            )
        mixed = lax.psum_scatter(
            jnp.dot(
                jnp.concatenate(attended, axis=1),
                out_w[layer],
                preferred_element_type=jnp.float32,
            ).astype(jnp.bfloat16),
            "tp",
            scatter_dimension=0,
            tiled=True,
        ).astype(jnp.float32)
        hidden_state = hidden_state + mixed
    return unit_rows(hidden_state) * final_gain.astype(jnp.float32)


def solution(mesh):
    in_specs = (
        P(("sp", "tp"), None),
        P(("sp", "tp"), None),
        P(),
        P(),
        P(None, None, "tp"),
        P(None, None, "tp"),
        P(None, None, "tp"),
        P(None, "tp", None),
        P(None, "tp"),
        P(),
    )
    out_specs = P(("sp", "tp"), None)
    return jax.shard_map(
        per_device, mesh=mesh, in_specs=in_specs, out_specs=out_specs, check_vma=False
    )
```

time: 715 us -> 372 us (0.52)
  waiting for transfers between devices: 508 us -> 168 us
  Pallas kernels: 0 us -> 112 us
  matrix products: 101 us -> 40.5 us
  local copies, waits for them, and re-layouts: 57.2 us -> 12 us
    all_gather x5 -> x1, waiting for transfers between devices: 462 us -> 103 us  [per_device(): lax.all_gather(unit_rows(source).astype(jnp.bfloat16), ('sp', 'tp'), axis...]
    pallas_call x0 -> x2, Pallas kernels: none -> 112 us  [attend(): pl.pallas_call(functools.partial(attend_kernel, rows), grid=(positions //...]
    dot_general x12 -> x20, matrix products: 101 us -> 40.5 us  [the longest x2 13.6 us: per_device(): jnp.dot(jnp.concatenate(attended, axis=1), out_w[layer], preferred_elemen...]
    reshape x6 -> x0, local copies, waits for them, and re-layouts: 56.3 us -> none  [the longest x2 29.4 us: per_device(): lax.all_gather(key_rows, 'sp', axis=0, tiled=True)]
    reduce_sum x2 -> x0, other arithmetic: 17.2 us -> none  [per_device(): row_total = jnp.sum(exponent, axis=-1)]
    reduce_scatter x2, waiting for transfers between devices: 36.5 us -> 48.1 us  [per_device(): lax.psum_scatter(jnp.dot(jnp.concatenate(attended, axis=1), out_w[layer],...]
    squeeze x0 -> x2, local copies, waits for them, and re-layouts: none -> 10.3 us  [the longest x1 6.58 us: per_device(): key_w[layer][:, columns]]
    all_gather x2, waiting for transfers between devices: 8.2 us -> 16.8 us  [per_device(): lax.all_gather(normed, 'tp', axis=0, tiled=True)]
  transfers between devices with their start and end apart: 9 -> 5, of which waited for: 9 -> 4; matrix products, arithmetic and copies ran while one was open for 15% -> 9% of each run, Pallas kernels for 0% -> 0%
where the time goes in v1:
time: 372 us
  waiting for transfers between devices  168 us (45%)
  Pallas kernels  112 us (30%)
  matrix products  40.5 us (11%)
  other arithmetic  25.4 us (7%)
  between operations  13.4 us (4%)
  local copies, waits for them, and re-layouts  12 us (3%)
    pallas_call x2, Pallas kernels, attend(): pl.pallas_call(functools.partial(attend_kernel, rows), grid=(positions //...  112 us
    all_gather x1, waiting for transfers between devices, per_device(): lax.all_gather(unit_rows(source).astype(jnp.bfloat16), ('sp', 'tp'), axis...  103 us
    reduce_scatter x2, waiting for transfers between devices, per_device(): lax.psum_scatter(jnp.dot(jnp.concatenate(attended, axis=1), out_w[layer],...  48.1 us
    all_gather x2, waiting for transfers between devices, per_device(): lax.all_gather(normed, 'tp', axis=0, tiled=True)  16.8 us
    dot_general x2, matrix products, per_device(): jnp.dot(jnp.concatenate(attended, axis=1), out_w[layer], preferred_elemen...  13.6 us
    dot_general x2, matrix products, per_device(): jnp.dot(lax.all_gather(normed, 'tp', axis=0, tiled=True), query_w[layer],...  12.3 us
    dot_general x8, matrix products, per_device(): jnp.dot(own, value_w[layer][:, columns], preferred_element_type=jnp.float32)  8.58 us
  transfers between devices with their start and end apart: 5, of which 4 were waited for; matrix products, arithmetic and copies ran while one was open for 9% of the time, Pallas kernels for 0%

profile of v1, /device:TPU:0, one launch (start us, length us, event | category | flops | bytes accessed | tf_op | source)
XLA Modules:
  0.0 371.6 jit_solution(17510046657952008814)
XLA Ops:
  6.5 0.0 all-gather.4.cloned.1.call-start
  6.5 0.8 slice_convert_fusion.1
  7.3 1.1 fusion.112
  8.4 1.8 fusion.114
  10.2 0.0 all-gather.4.cloned.1.call-update
  10.3 0.0 all-gather.6.cloned.1.call-start
  10.3 1.2 fusion.80
  11.6 2.0 fusion.81
  13.6 0.0 all-gather.6.cloned.1.call-update
  13.6 0.0 reduce-scatter.3.cloned.1.call-start
  13.6 0.8 slice_multiply_fusion.1
  14.4 0.7 fusion.125
  15.1 0.8 slice_convert_fusion
  15.9 0.0 slice-start
  15.9 6.1 %broadcast_multiply_fusion.3 = (f32[1,2048]{1,0:T(1,128)S(1)}, f32[1,2048]{1,0:T(1,128)S(1)}, f32[1,2048]{1,0:T(1,128)S(1)}, f32[1,2048]{1,0:T(1,128)S(1)}, f32[...) fusion(f32[]{:T(128)} %bitcast.17, bf16[2,2048]{1,0:T(2,128)(2,1)} %param.13, ...), kind=kLoop, calls=%fused_computation.138 | loop fusion | flops 20480 | bytes 73760 | tf_op jit(solution)/shard_map/mul | solution.py:124
  22.0 0.0 slice-start.1
  22.0 6.6 %slice_bitcast_fusion.3 = (bf16[2048,1024]{1,0:T(8,128)(2,1)}, bf16[2048,1024]{1,0:T(8,128)(2,1)}) fusion(bf16[2,2048,1024]{2,1,0:T(8,128)(2,1)} %param.15), kind=kLoop, calls=%fused_computation.17 | loop fusion | bytes 16777216 | tf_op jit(solution)/shard_map/squeeze | solution.py:120
  28.6 0.0 slice-done
  28.6 0.2 slice-done.1
  28.8 3.7 %slice_bitcast_fusion.2 = (bf16[2048,1024]{1,0:T(8,128)(2,1)}, bf16[2048,1024]{1,0:T(8,128)(2,1)}) fusion(bf16[2,2048,1024]{2,1,0:T(8,128)(2,1)S(1)} %bitcast.51), kind=kLoop, calls=%fused_computation.16 | loop fusion | bytes 16777216 | tf_op jit(solution)/shard_map/squeeze | solution.py:136
  32.5 6.2 %fusion.20 = bf16[256,2048]{1,0:T(8,128)(2,1)S(1)} fusion(bf16[256,2048]{1,0:T(8,128)(2,1)} %all-gather.4.cloned.1.call-done, bf16[2,2048,2048]{2,1,0:T(8,128)(2,1)} %param.14), kind=kOutput, calls=%fused_computation.34 | convolution fusion | flops 2148007936 | bytes 10485760 | tf_op jit(solution)/shard_map/dot_general | solution.py:106
  38.7 0.0 copy-done.5
  38.7 0.7 fusion.12
  39.4 0.7 fusion.13
  40.2 0.7 fusion.14
  41.0 0.7 fusion.15
  41.7 2.3 pad_maximum_fusion.query_ref
  44.0 103.3 %all-gather.6.cloned.1.call-done.source_ref = bf16[4096,2048]{1,0:T(8,128)(2,1)} async-done(((bf16[128,2048]{1,0:T(8,128)(2,1)}), bf16[4096,2048]{1,0:T(8,128)(2,1)}) %all-gather.6.cloned.1.call-update) | async-done | bytes 16777232 | tf_op jit(solution)/shard_map/all_gather | solution.py:97
  147.3 56.0 %shard_map.100 = bf16[1024,2048]{1,0:T(8,128)(2,1)} custom-call(bf16[1024,2048]{1,0:T(8,128)(2,1)} %pad_maximum_fusion.query_ref, bf16[4096,2048]{1,0:T(8,128)(2,1)} %all-gather.6.cloned.1.call-done.source_ref), custom_call_target="tpu_custom_call" | custom-call | flops 34359738368 | bytes 16777216 | tf_op jit(solution)/shard_map/pallas_call | solution.py:65
  203.3 0.0 copy-done.4
  203.3 2.1 fusion.56
  205.4 0.4 copy-done.8
  205.8 0.7 fusion.59
  206.5 0.7 fusion.62
  207.3 0.7 fusion.65
  208.0 0.0 copy-start
  208.0 6.8 %fusion.23 = bf16[256,2048]{1,0:T(8,128)(2,1)} fusion(bf16[2,2048,2048]{2,1,0:T(8,128)(2,1)} %param.17, bf16[256,512]{1,0:T(8,128)(2,1)S(1)} %fusion.65, bf16[256,512]{1,0:T(8,128)(2,1)S(1)} %fusion.62, bf16[256,512]{1,0:T(8,128)(2,1)S(1)} %fusion.59, bf16[256,512]{1,0:T(8,128)(2,1)S(1)} %fusion.56), kind=kOutput, calls=%fused_computation.35 | convolution fusion | flops 2152202240 | bytes 10485760 | tf_op jit(solution)/shard_map/dot_general | solution.py:140
  214.8 0.0 reduce-scatter.3.cloned.1.call-update
  214.8 0.0 all-gather.8.cloned.1.call-start
  214.9 23.1 %reduce-scatter.3.cloned.1.call-done = bf16[64,2048]{1,0:T(8,128)(2,1)} async-done(((bf16[256,2048]{1,0:T(8,128)(2,1)}), bf16[64,2048]{1,0:T(8,128)(2,1)}) %reduce-scatter.3.cloned.1.call-update) | async-done | bytes 262160 | tf_op jit(solution)/shard_map/reduce_scatter | solution.py:139
  238.0 1.1 multiply_reduce_fusion.1
  239.2 1.8 multiply_convert_fusion.16
  241.0 0.0 all-gather.8.cloned.1.call-update
  241.0 0.0 reduce-scatter.5.cloned.1.call-start
  241.0 16.8 %all-gather.8.cloned.1.call-done = bf16[256,2048]{1,0:T(8,128)(2,1)} async-done(((bf16[64,2048]{1,0:T(8,128)(2,1)}), bf16[256,2048]{1,0:T(8,128)(2,1)}) %all-gather.8.cloned.1.call-update) | async-done | bytes 1048592 | tf_op jit(solution)/shard_map/all_gather | solution.py:107
  257.8 6.2 %fusion.26 = bf16[256,2048]{1,0:T(8,128)(2,1)S(1)} fusion(bf16[256,2048]{1,0:T(8,128)(2,1)} %all-gather.8.cloned.1.call-done, bf16[2,2048,2048]{2,1,0:T(8,128)(2,1)} %param.14), kind=kOutput, calls=%fused_computation.36 | convolution fusion | flops 2148007936 | bytes 10485760 | tf_op jit(solution)/shard_map/dot_general | solution.py:106
  264.0 0.0 copy-done.3
  264.0 0.7 fusion.16
  264.8 0.7 fusion.17
  265.5 0.7 fusion.18
  266.3 0.7 fusion.19
  267.0 2.5 pad_maximum_fusion.1.query_ref
  269.5 56.0 %shard_map.101 = bf16[1024,2048]{1,0:T(8,128)(2,1)} custom-call(bf16[1024,2048]{1,0:T(8,128)(2,1)} %pad_maximum_fusion.1.query_ref, bf16[4096,2048]{1,0:T(8,128)(2,1)} %all-gather.6.cloned.1.call-done.source_ref), custom_call_target="tpu_custom_call" | custom-call | flops 34359738368 | bytes 16777216 | tf_op jit(solution)/shard_map/pallas_call | solution.py:65
  325.5 2.1 fusion.68
  327.6 0.4 copy-done.7
  328.0 0.7 fusion.71
  328.8 0.7 fusion.74
  329.5 0.7 fusion.77
  330.3 0.0 copy-start.6
  330.3 6.7 %fusion.29 = bf16[256,2048]{1,0:T(8,128)(2,1)} fusion(bf16[2,2048,2048]{2,1,0:T(8,128)(2,1)} %param.17, bf16[256,512]{1,0:T(8,128)(2,1)S(1)} %fusion.77, bf16[256,512]{1,0:T(8,128)(2,1)S(1)} %fusion.74, bf16[256,512]{1,0:T(8,128)(2,1)S(1)} %fusion.71, bf16[256,512]{1,0:T(8,128)(2,1)S(1)} %fusion.68), kind=kOutput, calls=%fused_computation.37 | convolution fusion | flops 2152202240 | bytes 10485760 | tf_op jit(solution)/shard_map/dot_general | solution.py:140
  337.0 0.0 reduce-scatter.5.cloned.1.call-update
  337.1 24.9 %reduce-scatter.5.cloned.1.call-done = bf16[64,2048]{1,0:T(8,128)(2,1)} async-done(((bf16[256,2048]{1,0:T(8,128)(2,1)}), bf16[64,2048]{1,0:T(8,128)(2,1)}) %reduce-scatter.5.cloned.1.call-update) | async-done | bytes 262160 | tf_op jit(solution)/shard_map/reduce_scatter | solution.py:139
  362.0 1.2 multiply_reduce_fusion
  363.2 1.9 multiply_multiply_fusion
  (18 shorter events, 0.1 us)
Async XLA Ops:
  6.5 26.0 %all-gather.4.cloned.1.call-start = ((), (), s32[]{:S(2)}) async-start(), calls=%async_computation.2 | async-start | bytes 1310720 | tf_op jit(solution)/shard_map/all_gather | solution.py:107
  10.3 137.0 %all-gather.6.cloned.1.call-start = ((), (), s32[]{:S(2)}) async-start(), calls=%async_computation.3 | async-start | bytes 17301504 | tf_op jit(solution)/shard_map/all_gather | solution.py:97
  13.6 224.4 %reduce-scatter.3.cloned.1.call-start = ((), (), s32[]{:S(2)}) async-start(), calls=%async_computation.4 | async-start | bytes 1310720 | tf_op jit(solution)/shard_map/reduce_scatter | solution.py:139
  15.9 12.7 %slice-start = ((s8[8388608]{0:T(1024)(128)(4,1)}), s8[4194304]{0:T(1024)(128)(4,1)S(1)}, s32[]{:S(2)}) async-start(s8[8388608]{0:T(1024)(128)(4,1)} %bitcast.50), calls=%async_computation.7 | async-start | bytes 8388608
  22.0 6.8 %slice-start.1 = ((s8[8388608]{0:T(1024)(128)(4,1)}), s8[4194304]{0:T(1024)(128)(4,1)S(1)}, s32[]{:S(2)}) async-start(s8[8388608]{0:T(1024)(128)(4,1)} %bitcast.50), calls=%async_computation.8 | async-start | bytes 8388608
  32.5 6.2 %copy-start.5 = (bf16[2048,1024]{1,0:T(8,128)(2,1)S(1)}, bf16[2048,1024]{1,0:T(8,128)(2,1)}, u32[]{:S(2)}) copy-start(bf16[2048,1024]{1,0:T(8,128)(2,1)} %get-tuple-element.5) | copy-start | bytes 12582916
  147.3 56.0 %copy-start.4 = (bf16[2048,1024]{1,0:T(8,128)(2,1)S(1)}, bf16[2048,1024]{1,0:T(8,128)(2,1)}, u32[]{:S(2)}) copy-start(bf16[2048,1024]{1,0:T(8,128)(2,1)} %get-tuple-element.7) | copy-start | bytes 12582916
  203.3 2.5 copy-start.8
  208.0 30.0 %copy-start = (bf16[64,2048]{1,0:T(8,128)(2,1)S(1)}, bf16[64,2048]{1,0:T(8,128)(2,1)}, u32[]{:S(2)}) copy-start(bf16[64,2048]{1,0:T(8,128)(2,1)} %param.10) | copy-start | bytes 786436
  214.8 43.0 %all-gather.8.cloned.1.call-start = ((), (), s32[]{:S(2)}) async-start(), calls=%async_computation.5 | async-start | bytes 1310720 | tf_op jit(solution)/shard_map/all_gather | solution.py:107
  241.0 121.0 %reduce-scatter.5.cloned.1.call-start = ((), (), s32[]{:S(2)}) async-start(), calls=%async_computation.6 | async-start | bytes 1310720 | tf_op jit(solution)/shard_map/reduce_scatter | solution.py:139
  257.8 6.2 %copy-start.3 = (bf16[2048,1024]{1,0:T(8,128)(2,1)S(1)}, bf16[2048,1024]{1,0:T(8,128)(2,1)}, u32[]{:S(2)}) copy-start(bf16[2048,1024]{1,0:T(8,128)(2,1)} %get-tuple-element.6) | copy-start | bytes 12582916
  269.5 56.0 %copy-start.2 = (bf16[2048,1024]{1,0:T(8,128)(2,1)S(1)}, bf16[2048,1024]{1,0:T(8,128)(2,1)}, u32[]{:S(2)}) copy-start(bf16[2048,1024]{1,0:T(8,128)(2,1)} %get-tuple-element.8) | copy-start | bytes 12582916
  325.5 2.5 copy-start.7
  330.3 6.8 %copy-start.6 = (bf16[2048]{0:T(1024)(128)(2,1)S(1)}, bf16[2048]{0:T(1024)(128)(2,1)}, u32[]{:S(2)}) copy-start(bf16[2048]{0:T(1024)(128)(2,1)} %param.19) | copy-start | bytes 12292
  330.3 31.7 %copy-start.1 = (bf16[64,2048]{1,0:T(8,128)(2,1)S(1)}, bf16[64,2048]{1,0:T(8,128)(2,1)}, u32[]{:S(2)}) copy-start(bf16[64,2048]{1,0:T(8,128)(2,1)} %reduce-scatter.3.cloned.1.call-done) | copy-start | bytes 786436
Sparse Core Ops, SparseCore 0:
  10.4 19.4 all-gather.3
  32.7 114.5 all-gather.5
  215.0 23.0 reduce-scatter.2
  241.1 16.6 all-gather.7
  337.2 24.7 reduce-scatter.4
